TPU v7x, 32 devices: a whole 2x2x4 slice. The times are simulated.
32 devices in a mesh: sp: 4 (over x, core), dp: 8 (over z, y).
Axes of the slice: x: 2, y: 2, z: 4, core: 2. Of those that a mesh axis runs over, the one named last changes fastest.
Arguments:
- tokens: bfloat16 [8, 1536, 2048], P('dp', 'sp'), may hold values from -6 to 6
- w_value: bfloat16 [2048, 1024], P('dp'), may hold values from -0.125 to 0.125
- w_gate: bfloat16 [2048, 1024], P('dp'), may hold values from -0.125 to 0.125
- conv_taps: bfloat16 [31, 1024], replicated, may hold values from -1 to 1
- norm_gain: bfloat16 [1024], replicated, may hold values from 0.099609375 to 1.8984375
- w_out: bfloat16 [1024, 2048], P(None, 'dp'), may hold values from -0.1875 to 0.1875
Outputs:
- mixed: bfloat16 [8, 1536, 2048], P('dp', 'sp')
All inputs are finite; a program needn't handle non-finite values.
Results may differ from a plain program's by a relative error of at most 0.013.
Values may be sent and summed in bfloat16 or wider, within the bound.
No kernel may reach another device: no remote copies, remote signals or barrier semaphores. Data moves between devices by JAX's collectives and lax.ppermute only.
A program may use at most 64 MiB of HBM per device.

v0:
```python
import jax
import jax.numpy as jnp
from jax import lax
from jax.sharding import PartitionSpec as P

EPSILON = 1e-06


def passed_along(x, axis, by):
    length = lax.axis_size(axis)
    pairs = [(i, i + by) for i in range(length) if 0 <= i + by < length]
    return lax.ppermute(x, axis, pairs)


def depthwise_conv(signal, local_taps, left_pad):
    kernel_form = jnp.transpose(local_taps)[:, None, :]
    result = lax.conv_general_dilated(
        signal[None],
        kernel_form,
        (1,),
        [(left_pad, 0)],
        dimension_numbers=("NCH", "OIH", "NCH"),
        feature_group_count=signal.shape[0],
        preferred_element_type=jnp.float32,
    )
    return result[0].astype(jnp.bfloat16)


def body(tokens, w_value, w_gate, conv_taps, norm_gain, w_out):
    seq_rows = tokens[0]
    tok_count = seq_rows.shape[0]
    kernel_len = conv_taps.shape[0]
    value_sum = jnp.einsum(
        "dc,td->ct",
        lax.all_gather(w_value, "dp", axis=0, tiled=True),
        seq_rows,
        preferred_element_type=jnp.float32,
    )
    gate_sum = jnp.einsum(
        "dc,td->ct",
        lax.all_gather(w_gate, "dp", axis=0, tiled=True),
        seq_rows,
        preferred_element_type=jnp.float32,
    )
    gated = (value_sum * jax.nn.sigmoid(gate_sum)).astype(jnp.bfloat16)
    last_rows = gated[:, tok_count - (kernel_len - 1) :]
    earlier = passed_along(last_rows, "sp", 1)
    extended = jnp.concatenate([earlier, gated], axis=1)
    conv_out = depthwise_conv(extended, conv_taps, 0)
    wide = conv_out.astype(jnp.float32)
    chan_mean = jnp.mean(wide, 0, keepdims=True)
    centred = wide - chan_mean
    chan_var = jnp.mean(centred * centred, 0, keepdims=True)
    normed = centred * lax.rsqrt(chan_var + EPSILON) * norm_gain.astype(jnp.float32)[:, None]
    activated = (normed * jax.nn.sigmoid(normed)).astype(jnp.bfloat16)
    projected = jnp.einsum(
        "ct,cd->td",
        activated,
        lax.all_gather(w_out, "dp", axis=1, tiled=True),
        preferred_element_type=jnp.float32,
    ).astype(jnp.bfloat16)
    return projected[None]


def solution(mesh):
    placed = (P("dp", "sp", None), P("dp", None), P("dp", None), P(), P(), P(None, "dp"))
    return jax.shard_map(
        body, mesh=mesh, in_specs=placed, out_specs=P("dp", "sp", None), check_vma=False
    )
```

profile of v0, /device:TPU:0, one launch (start us, length us, event | category | flops | bytes accessed | tf_op | source)
XLA Modules:
  0.0 246.4 jit_solution(6799378059922831921)
XLA Ops:
  6.5 0.0 copy-start
  6.5 0.0 all-gather.6.cloned.1.call-start
  6.5 0.7 all-gather.6.cloned.1.call-update
  7.3 0.0 all-gather.4.cloned.1.call-start
  7.3 0.7 all-gather.4.cloned.1.call-update
  8.0 0.0 all-gather.8.cloned.1.call-start
  8.1 0.7 all-gather.8.cloned.1.call-update
  8.7 76.3 %all-gather.6.cloned.1.call-done = bf16[2048,1024]{1,0:T(8,128)(2,1)} async-done(((bf16[256,1024]{1,0:T(8,128)(2,1)}), bf16[2048,1024]{1,0:T(8,128)(2,1)}) %all-gather.6.cloned.1.call-update) | async-done | bytes 4194320 | tf_op jit(solution)/shard_map/all_gather | solution.py:41
  85.0 0.0 copy-done
  85.0 4.0 %fusion.4 = f32[1024,384]{0,1:T(8,128)S(1)} fusion(bf16[2048,1024]{1,0:T(8,128)(2,1)} %all-gather.6.cloned.1.call-done, bf16[1,384,2048]{2,1,0:T(8,128)(2,1)S(1)} %copy-done), kind=kOutput, calls=%fused_computation.8 | convolution fusion | flops 1610612736 | bytes 7340032 | tf_op jit(solution)/shard_map/dc,td->ct/dot_general | solution.py:39
  89.0 0.0 copy-start.1
  89.0 69.5 %all-gather.4.cloned.1.call-done = bf16[2048,1024]{1,0:T(8,128)(2,1)} async-done(((bf16[256,1024]{1,0:T(8,128)(2,1)}), bf16[2048,1024]{1,0:T(8,128)(2,1)}) %all-gather.4.cloned.1.call-update) | async-done | bytes 4194320 | tf_op jit(solution)/shard_map/all_gather | solution.py:35
  158.5 4.1 %multiply_convert_fusion.1 = bf16[1024,384]{0,1:T(8,128)(2,1)S(1)} fusion(f32[1024,384]{0,1:T(8,128)S(1)} %fusion.4, bf16[2048,1024]{1,0:T(8,128)(2,1)} %all-gather.4.cloned.1.call-done, bf16[1,384,2048]{2,1,0:T(8,128)(2,1)S(1)} %copy-done), kind=kOutput, calls=%fused_computation.12 | convolution fusion | flops 1612578816 | bytes 8126464 | tf_op jit(solution)/shard_map/dc,td->ct/dot_general | solution.py:33
  162.6 1.3 collective-permute-start
  163.9 0.0 copy-done.1
  163.9 0.9 collective-permute-done
  164.8 0.2 maximum_bitcast_fusion
  165.0 0.1 pad
  165.0 0.2 reshape.17
  165.2 0.0 copy-start.2
  165.2 0.0 copy-start.3
  165.2 0.5 copy.12
  165.7 0.1 slice.7
  165.8 0.2 copy-done.2
  166.0 0.0 copy-done.3
  166.0 3.8 %fusion.17 = f32[8,52,1024]{2,0,1:T(8,128)S(1)} fusion(bf16[1024,1,7,30]{0,2,3,1:T(8,128)(2,1)S(1)} %slice.7, bf16[1024,1,8,52]{0,2,3,1:T(8,128)(2,1)S(1)} %copy.12, pred[8,52]{0,1:T(8,128)(4,1)S(1)} %copy-done.3, bf16[1024,1,31]{0,2,1:T(8,128)(2,1)S(1)} %bitcast.35), kind=kOutput, calls=%fused_computation.20 | convolution fusion | flops 31719424 | bytes 3049888 | tf_op jit(solution)/shard_map/conv_general_dilated | solution.py:17
  169.8 2.2 copy.14
  172.1 1.6 reshape.21
  173.7 0.2 slice_reduce_fusion
  173.8 0.3 multiply_reduce_fusion
  174.1 60.3 %all-gather.8.cloned.1.call-done = bf16[1024,2048]{1,0:T(8,128)(2,1)} async-done(((bf16[1024,256]{1,0:T(8,128)(2,1)}), bf16[1024,2048]{1,0:T(8,128)(2,1)}) %all-gather.8.cloned.1.call-update) | async-done | bytes 4194320 | tf_op jit(solution)/shard_map/all_gather | solution.py:59
  234.5 5.5 %fusion.1 = bf16[1,384,2048]{2,1,0:T(8,128)(2,1)} fusion(bf16[1024,2048]{1,0:T(8,128)(2,1)} %all-gather.8.cloned.1.call-done, f32[1,416,1024]{2,1,0:T(8,128)S(1)} %reshape.21, f32[1024]{0:T(1024)S(1)} %convert_element_type.26, f32[384]{0:T(512)S(1)} %add_rsqrt_fusion, f32[384]{0:T(512)S(1)} %broadcast_multiply_fusion), kind=kOutput, calls=%fused_computation.3 | convolution fusion | flops 1614544896 | bytes 7348224 | tf_op jit(solution)/shard_map/ct,cd->td/dot_general | solution.py:56
  (4 shorter events, 0.0 us)
Async XLA Ops:
  6.5 78.5 %copy-start = (bf16[1,384,2048]{2,1,0:T(8,128)(2,1)S(1)}, bf16[1,384,2048]{2,1,0:T(8,128)(2,1)}, u32[]{:S(2)}) copy-start(bf16[1,384,2048]{2,1,0:T(8,128)(2,1)} %param.6) | copy-start | bytes 4718596
  6.5 78.5 %all-gather.6.cloned.1.call-start = ((), (), s32[]{:S(2)}) async-start(), calls=%async_computation.1 | async-start | bytes 4718592 | tf_op jit(solution)/shard_map/all_gather | solution.py:41
  7.3 151.2 %all-gather.4.cloned.1.call-start = ((), (), s32[]{:S(2)}) async-start(), calls=%async_computation | async-start | bytes 4718592 | tf_op jit(solution)/shard_map/all_gather | solution.py:35
  8.0 226.4 %all-gather.8.cloned.1.call-start = ((), (), s32[]{:S(2)}) async-start(), calls=%async_computation.2 | async-start | bytes 4718592 | tf_op jit(solution)/shard_map/all_gather | solution.py:59
  89.0 74.9 %copy-start.1 = (bf16[1024]{0:T(1024)(128)(2,1)S(1)}, bf16[1024]{0:T(1024)(128)(2,1)}, u32[]{:S(2)}) copy-start(bf16[1024]{0:T(1024)(128)(2,1)} %param.10) | copy-start | bytes 6148
  162.6 2.2 collective-permute-start
  165.2 0.8 copy-start.2
  165.2 0.8 copy-start.3
Sparse Core Ops, SparseCore 0:
  9.5 75.5 all-gather.5
  87.1 71.3 all-gather.3
  160.5 73.8 all-gather.7
where the time goes:
time: 247 us; the launch traced here: 246 us
  waiting for transfers between devices  209 us (85%)
  matrix products  17.3 us (7%)
  between operations  13.2 us (5%)
  local copies, waits for them, and re-layouts  4.87 us (2%)
    all_gather x1, waiting for transfers between devices, body(): lax.all_gather(w_gate, 'dp', axis=0, tiled=True)  76.3 us
    all_gather x1, waiting for transfers between devices, body(): lax.all_gather(w_value, 'dp', axis=0, tiled=True)  69.5 us
    all_gather x1, waiting for transfers between devices, body(): lax.all_gather(w_out, 'dp', axis=1, tiled=True)  60.3 us
    dot_general x1, matrix products, body(): jnp.einsum('ct,cd->td', activated, lax.all_gather(w_out, 'dp', axis=1, ti...  5.46 us
  transfers between devices with their start and end apart: 4, of which 4 were waited for; matrix products, arithmetic and copies ran while one was open for 7% of the time, Pallas kernels for 0%

commit v1 on v0

--- a/solution.py
+++ b/solution.py
@@ -30,12 +30,27 @@
     seq_rows = tokens[0]
     tok_count = seq_rows.shape[0]
     kernel_len = conv_taps.shape[0]
-    value_sum = jnp.einsum(
+    devices, position = (lax.axis_size("dp"), lax.axis_index("dp"))
+    left = [(i_2, (i_2 - 1) % devices) for i_2 in range(devices)]
+    rows = w_value.shape[0]
+    held = w_value
+    so_far = jnp.einsum(
         "dc,td->ct",
-        lax.all_gather(w_value, "dp", axis=0, tiled=True),
-        seq_rows,
+        held,
+        lax.dynamic_slice_in_dim(seq_rows, position * rows, held.shape[0], axis=1),
         preferred_element_type=jnp.float32,
     )
+    for step in range(1, devices):
+        held = lax.ppermute(held, "dp", left)
+        so_far = so_far + jnp.einsum(
+            "dc,td->ct",
+            held,
+            lax.dynamic_slice_in_dim(
+                seq_rows, (position + step) % devices * rows, held.shape[0], axis=1
+            ),
+            preferred_element_type=jnp.float32,
+        )
+    value_sum = so_far
     gate_sum = jnp.einsum(
         "dc,td->ct",
         lax.all_gather(w_gate, "dp", axis=0, tiled=True),

time: 247 us -> 226 us (0.915)
  waiting for transfers between devices: 209 us -> 139 us
  starting transfers between devices: 1.37 us -> 38.8 us
  matrix products: 17.3 us -> 28 us
    ppermute x0 -> x7, waiting for transfers between devices: none -> 101 us  [body(): held = lax.ppermute(held, 'dp', left)]
    all_gather x1, waiting for transfers between devices: 76.3 us -> 0.01 us  [body(): lax.all_gather(w_gate, 'dp', axis=0, tiled=True)]
    all_gather x1 -> x0, waiting for transfers between devices: 69.5 us -> none  [body(): lax.all_gather(w_value, 'dp', axis=0, tiled=True)]
    ppermute x0 -> x7, starting transfers between devices: none -> 37.2 us  [body(): held = lax.ppermute(held, 'dp', left)]
    all_gather x1, waiting for transfers between devices: 60.3 us -> 36.5 us  [body(): lax.all_gather(w_out, 'dp', axis=1, tiled=True)]
    dot_general x1 -> x8, matrix products: 4.05 us -> 14.6 us  [the longest x7 13.2 us: body(): jnp.einsum('dc,td->ct', held, lax.dynamic_slice_in_dim(seq_rows, (positio...]
  transfers between devices with their start and end apart: 4 -> 10, of which waited for: 4 -> 9; matrix products, arithmetic and copies ran while one was open for 7% -> 12% of each run, Pallas kernels for 0% -> 0%
where the time goes in v1:
time: 226 us; the launch traced here: 225 us
  waiting for transfers between devices  139 us (62%)
  starting transfers between devices  38.8 us (17%)
  matrix products  28 us (12%)
  between operations  13.6 us (6%)
  local copies, waits for them, and re-layouts  4.94 us (2%)
    ppermute x7, waiting for transfers between devices, body(): held = lax.ppermute(held, 'dp', left)  101 us
    ppermute x7, starting transfers between devices, body(): held = lax.ppermute(held, 'dp', left)  37.2 us
    all_gather x1, waiting for transfers between devices, body(): lax.all_gather(w_out, 'dp', axis=1, tiled=True)  36.5 us
    dot_general x7, matrix products, body(): jnp.einsum('dc,td->ct', held, lax.dynamic_slice_in_dim(seq_rows, (positio...  13.2 us
    dot_general x1, matrix products, body(): jnp.einsum('ct,cd->td', activated, lax.all_gather(w_out, 'dp', axis=1, ti...  5.43 us
  transfers between devices with their start and end apart: 10, of which 9 were waited for; matrix products, arithmetic and copies ran while one was open for 12% of the time, Pallas kernels for 0%

profile of v1, /device:TPU:0, one launch (start us, length us, event | category | flops | bytes accessed | tf_op | source)
XLA Modules:
  0.0 225.2 jit_solution(10830962315625716754)
XLA Ops:
  6.5 0.0 copy-start
  6.5 0.0 all-gather.3.cloned.1.call-start
  6.5 0.7 all-gather.3.cloned.1.call-update
  7.3 0.0 all-gather.5.cloned.1.call-start
  7.3 0.7 all-gather.5.cloned.1.call-update
  8.0 6.1 %collective-permute-start = (bf16[256,1024]{1,0:T(8,128)(2,1)}, bf16[256,1024]{1,0:T(8,128)(2,1)S(1)}, u32[]{:S(2)}, u32[]{:S(2)}) collective-permute-start(bf16[256,1024]{1,0:T(8,128)(2,1)} %param.7), channel_id=1, source_target_pairs={{0,7},{1,0},{2,1},{3,2},{4,3},{5,4},{6,5},{7,6},{8,15},{9,8},{10,9... | collective-permute-start | bytes 1572872 | tf_op jit(solution)/shard_map/ppermute | solution.py:44
  14.1 17.0 %collective-permute-done = bf16[256,1024]{1,0:T(8,128)(2,1)S(1)} collective-permute-done((bf16[256,1024]{1,0:T(8,128)(2,1)}, bf16[256,1024]{1,0:T(8,128)(2,1)S(1)}, u32[]{:S(2)}, u32[]{:S(2)}) %collective-permute-start) | collective-permute-done | bytes 524320 | tf_op jit(solution)/shard_map/ppermute | solution.py:44
  31.1 0.0 copy-start.9
  31.1 5.1 %collective-permute-start.1 = (bf16[256,1024]{1,0:T(8,128)(2,1)S(1)}, bf16[256,1024]{1,0:T(8,128)(2,1)S(1)}, u32[]{:S(2)}, u32[]{:S(2)}) collective-permute-start(bf16[256,1024]{1,0:T(8,128)(2,1)S(1)} %collective-permute-done), channel_id=1, source_target_pairs={{0,7},{1,0},{2,1},{3,2},{4,3},{5,4},{6,5},{7,6},{8,15},{9,8},{10,9... | collective-permute-start | bytes 1572872 | tf_op jit(solution)/shard_map/ppermute | solution.py:44
  36.2 17.4 %collective-permute-done.1 = bf16[256,1024]{1,0:T(8,128)(2,1)S(1)} collective-permute-done((bf16[256,1024]{1,0:T(8,128)(2,1)S(1)}, bf16[256,1024]{1,0:T(8,128)(2,1)S(1)}, u32[]{:S(2)}, u32[]{:S(2)}) %collective-permute-start.1) | collective-permute-done | bytes 524320 | tf_op jit(solution)/shard_map/ppermute | solution.py:44
  53.6 0.0 copy-done.9
  53.6 5.2 %collective-permute-start.2 = (bf16[256,1024]{1,0:T(8,128)(2,1)S(1)}, bf16[256,1024]{1,0:T(8,128)(2,1)}, u32[]{:S(2)}, u32[]{:S(2)}) collective-permute-start(bf16[256,1024]{1,0:T(8,128)(2,1)S(1)} %collective-permute-done.1), channel_id=1, source_target_pairs={{0,7},{1,0},{2,1},{3,2},{4,3},{5,4},{6,5},{7,6},{8,15},{9,8},{10,9... | collective-permute-start | bytes 1572872 | tf_op jit(solution)/shard_map/ppermute | solution.py:44
  58.8 21.3 %collective-permute-done.2 = bf16[256,1024]{1,0:T(8,128)(2,1)} collective-permute-done((bf16[256,1024]{1,0:T(8,128)(2,1)S(1)}, bf16[256,1024]{1,0:T(8,128)(2,1)}, u32[]{:S(2)}, u32[]{:S(2)}) %collective-permute-start.2) | collective-permute-done | bytes 524320 | tf_op jit(solution)/shard_map/ppermute | solution.py:44
  80.1 0.0 copy-done.7
  80.1 5.3 %collective-permute-start.3 = (bf16[256,1024]{1,0:T(8,128)(2,1)}, bf16[256,1024]{1,0:T(8,128)(2,1)S(1)}, u32[]{:S(2)}, u32[]{:S(2)}) collective-permute-start(bf16[256,1024]{1,0:T(8,128)(2,1)} %collective-permute-done.2), channel_id=1, source_target_pairs={{0,7},{1,0},{2,1},{3,2},{4,3},{5,4},{6,5},{7,6},{8,15},{9,8},{10,9... | collective-permute-start | bytes 1572872 | tf_op jit(solution)/shard_map/ppermute | solution.py:44
  85.4 0.0 copy-done
  85.4 1.4 fusion.35
  86.8 0.0 copy-done.10
  86.8 0.0 copy-start.8
  86.8 1.6 fusion.33
  88.5 19.0 %collective-permute-done.3 = bf16[256,1024]{1,0:T(8,128)(2,1)S(1)} collective-permute-done((bf16[256,1024]{1,0:T(8,128)(2,1)}, bf16[256,1024]{1,0:T(8,128)(2,1)S(1)}, u32[]{:S(2)}, u32[]{:S(2)}) %collective-permute-start.3) | collective-permute-done | bytes 524320 | tf_op jit(solution)/shard_map/ppermute | solution.py:44
  107.5 5.1 %collective-permute-start.4 = (bf16[256,1024]{1,0:T(8,128)(2,1)S(1)}, bf16[256,1024]{1,0:T(8,128)(2,1)S(1)}, u32[]{:S(2)}, u32[]{:S(2)}) collective-permute-start(bf16[256,1024]{1,0:T(8,128)(2,1)S(1)} %collective-permute-done.3), channel_id=1, source_target_pairs={{0,7},{1,0},{2,1},{3,2},{4,3},{5,4},{6,5},{7,6},{8,15},{9,8},{10,9... | collective-permute-start | bytes 1572872 | tf_op jit(solution)/shard_map/ppermute | solution.py:44
  112.5 0.0 copy-done.8
  112.5 1.5 fusion.31
  114.1 2.6 %fusion.29 = f32[384,1024]{1,0:T(8,128)} fusion(bf16[256,1024]{1,0:T(8,128)(2,1)} %collective-permute-done.2, bf16[1,384,2048]{2,1,0:T(8,128)(2,1)S(1)} %copy-done, s32[]{:T(128)S(6)} %select_n.61), kind=kOutput, calls=%fused_computation.33 | convolution fusion | flops 201326592 | bytes 2293764 | tf_op jit(solution)/shard_map/dc,td->ct/dot_general | solution.py:45
  116.7 8.4 %collective-permute-done.4 = bf16[256,1024]{1,0:T(8,128)(2,1)S(1)} collective-permute-done((bf16[256,1024]{1,0:T(8,128)(2,1)S(1)}, bf16[256,1024]{1,0:T(8,128)(2,1)S(1)}, u32[]{:S(2)}, u32[]{:S(2)}) %collective-permute-start.4) | collective-permute-done | bytes 524320 | tf_op jit(solution)/shard_map/ppermute | solution.py:44
  125.1 5.2 %collective-permute-start.5 = (bf16[256,1024]{1,0:T(8,128)(2,1)S(1)}, bf16[256,1024]{1,0:T(8,128)(2,1)}, u32[]{:S(2)}, u32[]{:S(2)}) collective-permute-start(bf16[256,1024]{1,0:T(8,128)(2,1)S(1)} %collective-permute-done.4), channel_id=1, source_target_pairs={{0,7},{1,0},{2,1},{3,2},{4,3},{5,4},{6,5},{7,6},{8,15},{9,8},{10,9... | collective-permute-start | bytes 1572872 | tf_op jit(solution)/shard_map/ppermute | solution.py:44
  130.2 1.5 fusion.27
  131.8 1.5 fusion.25
  133.3 11.0 %collective-permute-done.5 = bf16[256,1024]{1,0:T(8,128)(2,1)} collective-permute-done((bf16[256,1024]{1,0:T(8,128)(2,1)S(1)}, bf16[256,1024]{1,0:T(8,128)(2,1)}, u32[]{:S(2)}, u32[]{:S(2)}) %collective-permute-start.5) | collective-permute-done | bytes 524320 | tf_op jit(solution)/shard_map/ppermute | solution.py:44
  144.3 5.3 %collective-permute-start.6 = (bf16[256,1024]{1,0:T(8,128)(2,1)}, bf16[256,1024]{1,0:T(8,128)(2,1)}, u32[]{:S(2)}, u32[]{:S(2)}) collective-permute-start(bf16[256,1024]{1,0:T(8,128)(2,1)} %collective-permute-done.5), channel_id=1, source_target_pairs={{0,7},{1,0},{2,1},{3,2},{4,3},{5,4},{6,5},{7,6},{8,15},{9,8},{10,9... | collective-permute-start | bytes 1572872 | tf_op jit(solution)/shard_map/ppermute | solution.py:44
  149.7 2.6 %fusion.23 = f32[384,1024]{1,0:T(8,128)} fusion(bf16[256,1024]{1,0:T(8,128)(2,1)} %collective-permute-done.5, bf16[1,384,2048]{2,1,0:T(8,128)(2,1)S(1)} %copy-done, s32[]{:T(128)S(6)} %select_n.67), kind=kOutput, calls=%fused_computation.27 | convolution fusion | flops 201326592 | bytes 2293764 | tf_op jit(solution)/shard_map/dc,td->ct/dot_general | solution.py:45
  152.3 0.0 copy-start.4
  152.3 0.0 copy-start.5
  152.3 0.0 copy-start.6
  152.3 4.1 %fusion.2 = f32[1024,384]{0,1:T(8,128)S(1)} fusion(bf16[2048,1024]{1,0:T(8,128)(2,1)} %all-gather.3.cloned.1.call-done, bf16[1,384,2048]{2,1,0:T(8,128)(2,1)S(1)} %copy-done), kind=kOutput, calls=%fused_computation.6 | convolution fusion | flops 1610612736 | bytes 7340032 | tf_op jit(solution)/shard_map/dc,td->ct/dot_general | solution.py:54
  156.4 0.0 copy-start.11
  156.4 6.6 %collective-permute-done.6 = bf16[256,1024]{1,0:T(8,128)(2,1)} collective-permute-done((bf16[256,1024]{1,0:T(8,128)(2,1)}, bf16[256,1024]{1,0:T(8,128)(2,1)}, u32[]{:S(2)}, u32[]{:S(2)}) %collective-permute-start.6) | collective-permute-done | bytes 524320 | tf_op jit(solution)/shard_map/ppermute | solution.py:44
  163.0 0.0 copy-done.1
  163.0 0.0 copy-done.2
  163.0 0.0 copy-done.3
  163.0 0.0 copy-done.4
  163.0 0.0 copy-done.5
  163.0 0.0 copy-done.6
  163.0 1.8 fusion.4
  164.9 1.5 collective-permute-start.7
  166.4 0.0 copy-done.11
  166.4 0.7 collective-permute-done.7
  167.1 0.2 maximum_bitcast_fusion
  167.3 0.1 pad
  167.4 0.2 reshape.25
  167.5 0.0 copy-start.12
  167.5 0.0 copy-start.13
  167.5 0.5 copy.12
  168.0 0.1 slice.7
  168.1 0.2 copy-done.12
  168.4 0.0 copy-done.13
  168.4 3.8 %fusion.14 = f32[8,52,1024]{2,0,1:T(8,128)S(1)} fusion(bf16[1024,1,7,30]{0,2,3,1:T(8,128)(2,1)S(1)} %slice.7, bf16[1024,1,8,52]{0,2,3,1:T(8,128)(2,1)S(1)} %copy.12, pred[8,52]{0,1:T(8,128)(4,1)S(1)} %copy-done.13, bf16[1024,1,31]{0,2,1:T(8,128)(2,1)S(1)} %bitcast.66), kind=kOutput, calls=%fused_computation.19 | convolution fusion | flops 31719424 | bytes 3049888 | tf_op jit(solution)/shard_map/conv_general_dilated | solution.py:17
  172.2 2.2 copy.14
  174.4 1.6 reshape.29
  176.0 0.2 slice_reduce_fusion
  176.2 0.3 multiply_reduce_fusion
  176.5 36.5 %all-gather.5.cloned.1.call-done = bf16[1024,2048]{1,0:T(8,128)(2,1)} async-done(((bf16[1024,256]{1,0:T(8,128)(2,1)}), bf16[1024,2048]{1,0:T(8,128)(2,1)}) %all-gather.5.cloned.1.call-update) | async-done | bytes 4194320 | tf_op jit(solution)/shard_map/all_gather | solution.py:74
  212.9 5.4 %fusion.1 = bf16[1,384,2048]{2,1,0:T(8,128)(2,1)} fusion(bf16[1024,2048]{1,0:T(8,128)(2,1)} %all-gather.5.cloned.1.call-done, f32[1,416,1024]{2,1,0:T(8,128)S(1)} %reshape.29, f32[1024]{0:T(1024)S(1)} %convert_element_type.26, f32[384]{0:T(512)S(1)} %add_rsqrt_fusion, f32[384]{0:T(512)S(1)} %broadcast_multiply_fusion), kind=kOutput, calls=%fused_computation.3 | convolution fusion | flops 1614544896 | bytes 7348224 | tf_op jit(solution)/shard_map/ct,cd->td/dot_general | solution.py:71
  (10 shorter events, 0.0 us)
Async XLA Ops:
  6.5 78.9 %copy-start = (bf16[1,384,2048]{2,1,0:T(8,128)(2,1)S(1)}, bf16[1,384,2048]{2,1,0:T(8,128)(2,1)}, u32[]{:S(2)}) copy-start(bf16[1,384,2048]{2,1,0:T(8,128)(2,1)} %param.6) | copy-start | bytes 4718596
  6.5 145.7 %all-gather.3.cloned.1.call-start = ((), (), s32[]{:S(2)}) async-start(), calls=%async_computation | async-start | bytes 4718592 | tf_op jit(solution)/shard_map/all_gather | solution.py:56
  7.3 205.7 %all-gather.5.cloned.1.call-start = ((), (), s32[]{:S(2)}) async-start(), calls=%async_computation.1 | async-start | bytes 4718592 | tf_op jit(solution)/shard_map/all_gather | solution.py:74
  8.0 23.1 %collective-permute-start = (bf16[256,1024]{1,0:T(8,128)(2,1)}, bf16[256,1024]{1,0:T(8,128)(2,1)S(1)}, u32[]{:S(2)}, u32[]{:S(2)}) collective-permute-start(bf16[256,1024]{1,0:T(8,128)(2,1)} %param.7), channel_id=1, source_target_pairs={{0,7},{1,0},{2,1},{3,2},{4,3},{5,4},{6,5},{7,6},{8,15},{9,8},{10,9... | collective-permute-start | bytes 1572872 | tf_op jit(solution)/shard_map/ppermute | solution.py:44
  31.1 22.5 %copy-start.9 = (bf16[256,1024]{1,0:T(8,128)(2,1)}, bf16[256,1024]{1,0:T(8,128)(2,1)S(1)}, u32[]{:S(2)}) copy-start(bf16[256,1024]{1,0:T(8,128)(2,1)S(1)} %collective-permute-done) | copy-start | bytes 1572868
  31.1 22.5 %collective-permute-start.1 = (bf16[256,1024]{1,0:T(8,128)(2,1)S(1)}, bf16[256,1024]{1,0:T(8,128)(2,1)S(1)}, u32[]{:S(2)}, u32[]{:S(2)}) collective-permute-start(bf16[256,1024]{1,0:T(8,128)(2,1)S(1)} %collective-permute-done), channel_id=1, source_target_pairs={{0,7},{1,0},{2,1},{3,2},{4,3},{5,4},{6,5},{7,6},{8,15},{9,8},{10,9... | collective-permute-start | bytes 1572872 | tf_op jit(solution)/shard_map/ppermute | solution.py:44
  53.6 26.5 %copy-start.7 = (bf16[256,1024]{1,0:T(8,128)(2,1)}, bf16[256,1024]{1,0:T(8,128)(2,1)S(1)}, u32[]{:S(2)}) copy-start(bf16[256,1024]{1,0:T(8,128)(2,1)S(1)} %collective-permute-done.1) | copy-start | bytes 1572868
  53.6 26.5 %collective-permute-start.2 = (bf16[256,1024]{1,0:T(8,128)(2,1)S(1)}, bf16[256,1024]{1,0:T(8,128)(2,1)}, u32[]{:S(2)}, u32[]{:S(2)}) collective-permute-start(bf16[256,1024]{1,0:T(8,128)(2,1)S(1)} %collective-permute-done.1), channel_id=1, source_target_pairs={{0,7},{1,0},{2,1},{3,2},{4,3},{5,4},{6,5},{7,6},{8,15},{9,8},{10,9... | collective-permute-start | bytes 1572872 | tf_op jit(solution)/shard_map/ppermute | solution.py:44
  58.8 28.1 %copy-start.10 = (bf16[256,1024]{1,0:T(8,128)(2,1)S(1)}, bf16[256,1024]{1,0:T(8,128)(2,1)}, u32[]{:S(2)}) copy-start(bf16[256,1024]{1,0:T(8,128)(2,1)} %copy-done.9) | copy-start | bytes 1572868
  80.1 27.4 %collective-permute-start.3 = (bf16[256,1024]{1,0:T(8,128)(2,1)}, bf16[256,1024]{1,0:T(8,128)(2,1)S(1)}, u32[]{:S(2)}, u32[]{:S(2)}) collective-permute-start(bf16[256,1024]{1,0:T(8,128)(2,1)} %collective-permute-done.2), channel_id=1, source_target_pairs={{0,7},{1,0},{2,1},{3,2},{4,3},{5,4},{6,5},{7,6},{8,15},{9,8},{10,9... | collective-permute-start | bytes 1572872 | tf_op jit(solution)/shard_map/ppermute | solution.py:44
  86.8 25.7 %copy-start.8 = (bf16[256,1024]{1,0:T(8,128)(2,1)S(1)}, bf16[256,1024]{1,0:T(8,128)(2,1)}, u32[]{:S(2)}) copy-start(bf16[256,1024]{1,0:T(8,128)(2,1)} %copy-done.7) | copy-start | bytes 1572868
  107.5 17.6 %collective-permute-start.4 = (bf16[256,1024]{1,0:T(8,128)(2,1)S(1)}, bf16[256,1024]{1,0:T(8,128)(2,1)S(1)}, u32[]{:S(2)}, u32[]{:S(2)}) collective-permute-start(bf16[256,1024]{1,0:T(8,128)(2,1)S(1)} %collective-permute-done.3), channel_id=1, source_target_pairs={{0,7},{1,0},{2,1},{3,2},{4,3},{5,4},{6,5},{7,6},{8,15},{9,8},{10,9... | collective-permute-start | bytes 1572872 | tf_op jit(solution)/shard_map/ppermute | solution.py:44
  125.1 19.3 %collective-permute-start.5 = (bf16[256,1024]{1,0:T(8,128)(2,1)S(1)}, bf16[256,1024]{1,0:T(8,128)(2,1)}, u32[]{:S(2)}, u32[]{:S(2)}) collective-permute-start(bf16[256,1024]{1,0:T(8,128)(2,1)S(1)} %collective-permute-done.4), channel_id=1, source_target_pairs={{0,7},{1,0},{2,1},{3,2},{4,3},{5,4},{6,5},{7,6},{8,15},{9,8},{10,9... | collective-permute-start | bytes 1572872 | tf_op jit(solution)/shard_map/ppermute | solution.py:44
  144.3 18.7 %collective-permute-start.6 = (bf16[256,1024]{1,0:T(8,128)(2,1)}, bf16[256,1024]{1,0:T(8,128)(2,1)}, u32[]{:S(2)}, u32[]{:S(2)}) collective-permute-start(bf16[256,1024]{1,0:T(8,128)(2,1)} %collective-permute-done.5), channel_id=1, source_target_pairs={{0,7},{1,0},{2,1},{3,2},{4,3},{5,4},{6,5},{7,6},{8,15},{9,8},{10,9... | collective-permute-start | bytes 1572872 | tf_op jit(solution)/shard_map/ppermute | solution.py:44
  152.3 10.7 %copy-start.1 = (f32[384,1024]{1,0:T(8,128)S(1)}, f32[384,1024]{1,0:T(8,128)}, u32[]{:S(2)}) copy-start(f32[384,1024]{1,0:T(8,128)} %fusion.33) | copy-start | bytes 4718596
  152.3 10.7 %copy-start.2 = (f32[384,1024]{1,0:T(8,128)S(1)}, f32[384,1024]{1,0:T(8,128)}, u32[]{:S(2)}) copy-start(f32[384,1024]{1,0:T(8,128)} %fusion.31) | copy-start | bytes 4718596
  152.3 10.7 %copy-start.3 = (f32[384,1024]{1,0:T(8,128)S(1)}, f32[384,1024]{1,0:T(8,128)}, u32[]{:S(2)}) copy-start(f32[384,1024]{1,0:T(8,128)} %fusion.29) | copy-start | bytes 4718596
  152.3 10.7 %copy-start.4 = (f32[384,1024]{1,0:T(8,128)S(1)}, f32[384,1024]{1,0:T(8,128)}, u32[]{:S(2)}) copy-start(f32[384,1024]{1,0:T(8,128)} %fusion.27) | copy-start | bytes 4718596
  152.3 10.7 %copy-start.5 = (f32[384,1024]{1,0:T(8,128)S(1)}, f32[384,1024]{1,0:T(8,128)}, u32[]{:S(2)}) copy-start(f32[384,1024]{1,0:T(8,128)} %fusion.25) | copy-start | bytes 4718596
  152.3 10.7 %copy-start.6 = (f32[384,1024]{1,0:T(8,128)S(1)}, f32[384,1024]{1,0:T(8,128)}, u32[]{:S(2)}) copy-start(f32[384,1024]{1,0:T(8,128)} %fusion.23) | copy-start | bytes 4718596
  156.4 9.9 %copy-start.11 = (bf16[1024]{0:T(1024)(128)(2,1)S(1)}, bf16[1024]{0:T(1024)(128)(2,1)}, u32[]{:S(2)}) copy-start(bf16[1024]{0:T(1024)(128)(2,1)} %param.10) | copy-start | bytes 6148
  164.9 2.2 collective-permute-start.7
  167.5 0.8 copy-start.12
  167.5 0.8 copy-start.13
Sparse Core Ops, SparseCore 0:
  9.5 110.3 all-gather.2
  121.9 91.0 all-gather.4
